TPU v7x, 256 devices: a whole 4x4x8 slice. The times are simulated.
256 devices in a mesh: sp: 64 (over z, x, core), tp: 4 (over y).
Axes of the slice: x: 4, y: 4, z: 8, core: 2. Of those that a mesh axis runs over, the one named last changes fastest.
Arguments:
- stream: bfloat16 [32768, 2048], P(('sp', 'tp')), may hold values from -6 to 6
- queries: bfloat16 [32768, 512], P('sp', 'tp'), may hold values from -6 to 6
- key_rows: bfloat16 [32768, 512], P('sp', 'tp'), may hold values from -6 to 6
- values: bfloat16 [32768, 1024], P('sp', 'tp'), may hold values from -6 to 6
- out_gate: bfloat16 [32768, 1024], P('sp', 'tp'), may hold values from -6 to 6
- fwd_decay: float32 [32768, 512], P('sp', 'tp'), may hold values from -14 to 14
- bwd_decay: float32 [32768, 512], P('sp', 'tp'), may hold values from -14 to 14
- head_gain: float32 [1024], P('tp'), may hold values from 0.1 to 1.9
- out_proj: bfloat16 [1024, 2048], replicated, may hold values from -0.1875 to 0.1875
- mix_gain: float32 [2048], replicated, may hold values from 0.1 to 1.9
- ffn_gain: float32 [2048], replicated, may hold values from 0.1 to 1.9
- moe_gain: float32 [2048], replicated, may hold values from 0.1 to 1.9
- routes: int32 [32768, 2], P(('sp', 'tp')), may hold values from 0 to 63, all different within a row; in each aligned block of 128 rows (0 to 127, 128 to 255, ...) at most 6 rows name the same one
- route_weight: float32 [32768, 2], P(('sp', 'tp')), may hold values from 0.25 to 2.5
- expert_gate: bfloat16 [64, 2048, 1024], P('sp', None, 'tp'), may hold values from -0.125 to 0.125
- expert_up: bfloat16 [64, 2048, 1024], P('sp', None, 'tp'), may hold values from -0.125 to 0.125
- expert_down: bfloat16 [64, 1024, 2048], P('sp', 'tp'), may hold values from -0.1875 to 0.1875
- shared_gate: bfloat16 [2048, 512], P(None, 'tp'), may hold values from -0.125 to 0.125
- shared_up: bfloat16 [2048, 512], P(None, 'tp'), may hold values from -0.125 to 0.125
- shared_down: bfloat16 [512, 2048], P('tp'), may hold values from -0.25 to 0.25
Outputs:
- updated: bfloat16 [32768, 2048], P(('sp', 'tp'))
Inputs may be any that keep to these rules, and one draw needn't show every extreme that they name: `routes`: each row names 2 different experts. Among the rows of one device no expert is named more than 6 times, and in every draw some device names some expert exactly 6 times.
All inputs are finite; a program needn't handle non-finite values.
Results may differ from a plain program's by a relative error of at most 0.023.
Values may be sent and summed in bfloat16 or wider, within the bound.
No kernel may reach another device: no remote copies, remote signals or barrier semaphores. Data moves between devices by JAX's collectives and lax.ppermute only.
A program may use at most 128 MiB of HBM per device.

v0:
```python
import jax
import jax.numpy as jnp
from jax import lax
from jax.sharding import Mesh
from jax.sharding import PartitionSpec as P

KEY_CHANNELS = 64
DV = 128
BLK = 64
TOPK = 2
SP = ("sp_0", "sp_1", "sp_2")
SP_TP = ("sp_0", "sp_1", "sp_2", "tp")
EPS = 1e-06
GATE_NORM = 16.0
ROPE_BASE = 10000.0


def gathered_once(array, axis):
    leaves = jax.tree.leaves(array)
    sequence = sorted(range(len(leaves)), key=lambda k: -leaves[k].size)
    width = (1, *leaves[sequence[0]].shape)[-1]
    lines = [
        jnp.pad(leaves[k].reshape(-1), (0, -leaves[k].size % width)).reshape(-1, width)
        for k in sequence
    ]
    both, at, found = (lax.all_gather(jnp.concatenate(lines), axis), 0, {})
    for k, line in zip(sequence, lines):
        share = both[:, at : at + len(line)].reshape(len(both), -1)
        found[k] = share[:, : leaves[k].size].reshape(-1, *leaves[k].shape)
        at += len(line)
    numbers = iter(range(len(leaves)))
    return jax.tree.map(lambda _: found[next(numbers)], array)


def prefix(array, axis, combine, identity):
    length, position = (lax.axis_size(axis), lax.axis_index(axis))
    everything = gathered_once(
        jax.tree.map(
            lambda part, kind: part.astype(kind),
            array,
            jax.tree.map(lambda a: jnp.bfloat16 if a.dtype == jnp.float32 else a.dtype, array),
        ),
        axis,
    )
    start = jax.tree.map(
        lambda part, zero: jnp.broadcast_to(jnp.asarray(zero, part.dtype), part.shape),
        array,
        identity,
    )

    def step(k, before):
        reached = k < position
        new = combine(
            before, jax.tree.map(lambda part, own: part[k].astype(own.dtype), everything, array)
        )
        return jax.tree.map(lambda a, b: jnp.where(reached, a, b), new, before)

    return lax.fori_loop(0, length, step, start)


def neutral_like(array, identity):
    return jax.tree.map(
        lambda a, e: jnp.broadcast_to(jnp.asarray(e, a.dtype), a.shape), array, identity
    )


def entering(array, axes, combine, identity):
    before = start = neutral_like(array, identity)
    so_far = array
    for axis in reversed(axes):
        length, position = (lax.axis_size(axis), lax.axis_index(axis))
        pieces = gathered_once(
            jax.tree.map(
                lambda part, kind: part.astype(kind),
                so_far,
                jax.tree.map(lambda a: jnp.bfloat16 if a.dtype == jnp.float32 else a.dtype, array),
            ),
            axis,
        )
        inside, so_far = (start, start)
        for k in reversed(range(length)):
            passed = k > position
            so_far = combine(
                so_far, jax.tree.map(lambda part, own: part[k].astype(own.dtype), pieces, array)
            )
            inside = jax.tree.map(lambda new, old: jnp.where(passed, new, old), so_far, inside)
        before = combine(inside, before)
    return before


def normalize(tensor):
    return tensor * lax.rsqrt(jnp.mean(tensor * tensor, axis=-1, keepdims=True) + EPS)


def rotate(tensor, positions):
    half_width = tensor.shape[-1] // 2
    frequency = ROPE_BASE ** (-jnp.arange(half_width, dtype=jnp.float32) / half_width)
    angles = positions[:, None] * frequency[None, :]
    cosine = jnp.cos(angles)[:, None, :]
    sine_part = jnp.sin(angles)[:, None, :]
    front_half = tensor[..., :half_width]
    back_half = tensor[..., half_width:]
    return jnp.concatenate(
        [front_half * cosine - back_half * sine_part, front_half * sine_part + back_half * cosine],
        axis=-1,
    )


def blockwise(query_rows, key_data, value_matrix, log_decay, start_state):
    length, head_count, key_width = query_rows.shape
    value_width = value_matrix.shape[-1]
    block_count = length // BLK
    query_blocks = query_rows.reshape(block_count, BLK, head_count, key_width)
    key_blocks = key_data.reshape(block_count, BLK, head_count, key_width)
    value_blocks = value_matrix.reshape(block_count, BLK, head_count, value_width)
    cumul = jnp.cumsum(log_decay.reshape(block_count, BLK, head_count, key_width), axis=1)
    middle = cumul[:, BLK // 2 - 1 : BLK // 2]
    query_scaled = query_blocks * jnp.exp(cumul - middle)
    key_scaled = key_blocks * jnp.exp(middle - cumul)
    scores = jnp.einsum("nthk,nshk->nhts", query_scaled, key_scaled)
    lower_mask = jnp.arange(BLK)[:, None] >= jnp.arange(BLK)[None, :]
    scores = jnp.where(lower_mask, scores, 0.0)
    within = jnp.einsum("nhts,nshv->nthv", scores, value_blocks)
    last_cumul = cumul[:, -1:]
    query_in = query_blocks * jnp.exp(cumul)
    key_out = key_blocks * jnp.exp(last_cumul - cumul)
    block_decay = jnp.exp(last_cumul[:, 0])

    def advance(carried_state, pieces):
        query_segment, key_segment, value_segment, decay_segment = pieces
        across_blocks = jnp.einsum("asu,sun->asn", query_segment, carried_state)
        carried_state = carried_state * decay_segment[:, :, None] + jnp.einsum(
            "jco,jcm->com", key_segment, value_segment
        )
        return (carried_state, across_blocks)

    final_state, across_blocks = lax.scan(
        advance, start_state, (query_in, key_out, value_blocks, block_decay)
    )
    return ((within + across_blocks).reshape(length, head_count, value_width), final_state)


def readout(query_rows, log_decay, carried_state):
    cumul = jnp.cumsum(log_decay, axis=0)
    return jnp.einsum("asu,sun->asn", query_rows * jnp.exp(cumul), carried_state)


def compose(earlier, later):
    return (earlier[0] * later[0], earlier[1] * later[0][:, :, None] + later[1])


def feed_forward(row_data, gate_mat, up_mat, down_mat):
    hidden = (
        jax.nn.silu(jnp.dot(row_data, gate_mat, preferred_element_type=jnp.float32))
        * jnp.dot(row_data, up_mat, preferred_element_type=jnp.float32)
    ).astype(jnp.bfloat16)
    return jnp.dot(hidden, down_mat, preferred_element_type=jnp.float32)


def place_slots(route_block, experts):
    flat_ids = route_block.reshape(-1)
    onehot = (flat_ids[:, None] == jnp.arange(experts, dtype=jnp.int32)[None, :]).astype(jnp.int32)
    before = jnp.cumsum(onehot, axis=0) - onehot
    return (flat_ids, jnp.sum(before * onehot, axis=1))


def fill_slots(row_data, route_block, experts, capacity):
    flat_ids, slot_ids = place_slots(route_block, experts)
    token_ids = jnp.arange(flat_ids.shape[0], dtype=jnp.int32) // route_block.shape[1]
    buffer = jnp.zeros((experts, capacity, row_data.shape[1]), row_data.dtype)
    return buffer.at[flat_ids, slot_ids].set(row_data[token_ids])


def body(
    stream,
    queries,
    key_rows,
    values,
    out_gate,
    fwd_decay,
    bwd_decay,
    head_gain,
    out_proj,
    mix_gain,
    ffn_gain,
    moe_gain,
    routes,
    route_weight,
    expert_gate,
    expert_up,
    expert_down,
    shared_gate,
    shared_up,
    shared_down,
):
    tokens_here = stream.shape[0]
    span_rows = queries.shape[0]
    heads_here = queries.shape[1] // KEY_CHANNELS
    offset = lax.axis_index(SP) * span_rows
    positions = (offset + jnp.arange(span_rows, dtype=jnp.int32)).astype(jnp.float32)
    query_rows = rotate(
        queries.astype(jnp.float32).reshape(span_rows, heads_here, KEY_CHANNELS)
        * KEY_CHANNELS ** (-0.5),
        positions,
    )
    key_data = rotate(
        key_rows.astype(jnp.float32).reshape(span_rows, heads_here, KEY_CHANNELS), positions
    )
    value_matrix = values.astype(jnp.float32).reshape(span_rows, heads_here, DV)
    fwd_log = jax.nn.log_sigmoid(fwd_decay).reshape(span_rows, heads_here, KEY_CHANNELS) / GATE_NORM
    bwd_log = (
        jax.nn.log_sigmoid(bwd_decay[::-1]).reshape(span_rows, heads_here, KEY_CHANNELS) / GATE_NORM
    )
    query_back = query_rows[::-1]
    key_back = key_data[::-1]
    value_back = value_matrix[::-1]
    zero_state = jnp.zeros((heads_here, KEY_CHANNELS, DV), jnp.float32)
    identity = (jnp.ones((heads_here, KEY_CHANNELS), jnp.float32), zero_state)
    fwd_out, fwd_final = blockwise(query_rows, key_data, value_matrix, fwd_log, zero_state)
    bwd_out, bwd_final = blockwise(query_back, key_back, value_back, bwd_log, zero_state)
    fwd_summary = (jnp.exp(jnp.sum(fwd_log, axis=0)), fwd_final)
    bwd_summary = (jnp.exp(jnp.sum(bwd_log, axis=0)), bwd_final)
    fwd_carry = prefix(fwd_summary, SP, compose, identity)[1]
    bwd_carry = entering(bwd_summary, SP, compose, identity)[1]
    fwd_out = fwd_out + readout(query_rows, fwd_log, fwd_carry)
    bwd_out = bwd_out + readout(query_back, bwd_log, bwd_carry)
    combined = normalize(fwd_out + bwd_out[::-1]) * head_gain.reshape(heads_here, DV)
    head_mixed = (
        combined.reshape(span_rows, -1) * jax.nn.silu(out_gate.astype(jnp.float32))
    ).astype(jnp.bfloat16)
    mixed_out = lax.all_to_all(head_mixed, "tp", split_axis=0, concat_axis=1, tiled=True)
    projected = jnp.dot(mixed_out, out_proj, preferred_element_type=jnp.float32)
    residual = (stream.astype(jnp.float32) + normalize(projected) * mix_gain).astype(jnp.bfloat16)
    normed = (normalize(residual.astype(jnp.float32)) * ffn_gain).astype(jnp.bfloat16)
    experts = lax.axis_size(SP)
    groups = lax.axis_size("tp")
    capacity = max(2, 3 * tokens_here * TOPK // (2 * experts))
    model_width = normed.shape[1]
    arrived = lax.all_to_all(
        fill_slots(normed, routes, experts, capacity), SP, split_axis=0, concat_axis=0, tiled=True
    )
    fanned, shared_flat = (
        lax.all_gather(arrived.reshape(experts * capacity, model_width), "tp", axis=0, tiled=True),
        lax.all_gather(normed, "tp", axis=0, tiled=True),
    )
    routed_rows = fanned.reshape(groups, experts * capacity, model_width)
    shared_rows = shared_flat.reshape(groups, tokens_here, model_width)
    width_rows = experts * capacity + tokens_here
    number = width_rows * lax.axis_size("tp") // width_rows
    routed_part = routed_rows.reshape(number * experts * capacity, model_width)
    shared_part = shared_rows.reshape(number * tokens_here, model_width)
    routed_out = feed_forward(routed_part, expert_gate[0], expert_up[0], expert_down[0]).reshape(
        number, experts * capacity, model_width
    )
    shared_out = feed_forward(shared_part, shared_gate, shared_up, shared_down).reshape(
        number, tokens_here, model_width
    )
    summed = lax.psum_scatter(
        jnp.concatenate([routed_out, shared_out], axis=1)
        .reshape(width_rows * lax.axis_size("tp"), model_width)
        .astype(jnp.bfloat16),
        "tp",
        scatter_dimension=0,
        tiled=True,
    ).astype(jnp.float32)
    routed_done = (
        summed[: experts * capacity].astype(jnp.bfloat16).reshape(experts, capacity, model_width)
    )
    routed_back = lax.all_to_all(routed_done, SP, split_axis=0, concat_axis=0, tiled=True)
    shared_sum = summed[experts * capacity :]
    flat_ids, slot_ids = place_slots(routes, experts)
    picked = routed_back.reshape(experts * capacity, model_width)[flat_ids * capacity + slot_ids]
    picked = picked.astype(jnp.float32).reshape(tokens_here, TOPK, model_width)
    mixture = shared_sum + jnp.sum(picked * route_weight[:, :, None], axis=1)
    return (residual.astype(jnp.float32) + normalize(mixture) * moe_gain).astype(jnp.bfloat16)


def solution(mesh):
    finer = Mesh(mesh.devices.reshape(8, 4, 2, mesh.shape["tp"]), ("sp_0", "sp_1", "sp_2", "tp"))
    placed = (
        P(SP_TP, None),
        P(SP, "tp"),
        P(SP, "tp"),
        P(SP, "tp"),
        P(SP, "tp"),
        P(SP, "tp"),
        P(SP, "tp"),
        P("tp"),
        P(),
        P(),
        P(),
        P(),
        P(SP_TP, None),
        P(SP_TP, None),
        P(SP, None, "tp"),
        P(SP, None, "tp"),
        P(SP, "tp", None),
        P(None, "tp"),
        P(None, "tp"),
        P("tp", None),
    )
    return jax.shard_map(
        body, mesh=finer, in_specs=placed, out_specs=P(SP_TP, None), check_vma=False
    )
```

profile of v0, /device:TPU:2, one launch (start us, length us, event | category | flops | bytes accessed | tf_op | source)
XLA Modules:
  0.0 553.1 jit_solution(17728160664577737282)
XLA Ops:
  10.0 13.0 %fusion.178 = f32[8,64,2,64]{3,0,1,2:T(8,128)S(1)} fusion(f32[8,64,2,64]{3,0,1,2:T(8,128)S(1)} %copy.134), kind=kOutput, calls=%fused_computation.308 | output fusion | flops 4128768 | bytes 524288 | tf_op jit(solution)/shard_map/jit(cumsum)/reduce_window_sum | solution.py:116
  36.9 24.3 %while.40 = (s32[]{:T(128)}, f32[2,64,128]{2,1,0:T(8,128)S(1)}, f32[8,64,2,128]{3,1,2,0:T(8,128)}, f32[8,2,64]{2,0,1:T(8,128)S(1)}, f32[8,64,2,64]{3,0,1,2:T(8,1...) while((s32[]{:T(128)}, f32[2,64,128]{2,1,0:T(8,128)S(1)}, ...), condition=%wide.region_2.3_spmd.clone, body=%wide.region_1.2_spmd.clone.sunk | while | flops 4259843 | bytes 494192 | solution.py:137
  63.6 3.1 rev.15
  66.7 3.1 rev.17
  83.2 24.4 %while.42 = (s32[]{:T(128)}, f32[2,64,128]{2,1,0:T(8,128)S(1)}, f32[8,64,2,128]{3,1,2,0:T(8,128)}, f32[8,2,64]{2,0,1:T(8,128)S(1)}, f32[8,64,2,64]{3,0,1,2:T(8,1...) while((s32[]{:T(128)}, f32[2,64,128]{2,1,0:T(8,128)S(1)}, ...), condition=%wide.region_10.11_spmd.clone, body=%wide.region_9.10_spmd.clone.sunk | while | flops 4259843 | bytes 494192 | solution.py:137
  107.7 2.4 fusion.24
  116.6 12.1 %all-gather.6 = bf16[4,129,128]{2,1,0:T(8,128)(2,1)S(1)} all-gather(bf16[1,129,128]{2,1,0:T(8,128)(2,1)S(1)} %maximum_bitcast_fusion.2), channel_id=4, replica_groups=mesh['sp_0'=8,'sp_1'=4,'sp_2'=2,'tp'=4] {'sp_1'}, dimensions={0}, use_global_device_ids=true | all-gather | bytes 165120 | tf_op jit(solution)/shard_map/all_gather | solution.py:26
  129.3 28.6 %all-gather.7 = bf16[8,129,128]{2,1,0:T(8,128)(2,1)S(1)} all-gather(bf16[1,129,128]{2,1,0:T(8,128)(2,1)S(1)} %maximum_bitcast_fusion.3), channel_id=5, replica_groups=mesh['sp_0'=8,'sp_1'=4,'sp_2'=2,'tp'=4] {'sp_0'}, dimensions={0}, use_global_device_ids=true | all-gather | bytes 297216 | tf_op jit(solution)/shard_map/all_gather | solution.py:26
  162.3 2.4 reduce-window.24
  167.0 3.0 rev.19
  170.0 2.4 reduce-window.20
  176.4 8.8 %while.41 = (s32[]{:T(128)}, f32[2,64,128]{2,1,0:T(8,128)S(1)}, s32[]{:T(128)}, bf16[64,2,64]{2,1,0:T(2,128)(2,1)S(1)}, bf16[64,2,64,128]{3,2,1,0:T(8,128)(2,1)S(1)}, /*index=5*/s32[]{:T(128)}, s32[]{:T(128)}) while((s32[]{:T(128)}, f32[2,64,128]{2,1,0:T(8,128)S(1)}, s32[]{:T(128)}, bf16[64,2,64]{2,1,0:T(2,128)(2,1)S(1)}, ...), condition=%wide.region_5.6_spmd.clone, body=%wide.region_4.5_spmd.clone.sunk | while | flops 82052 | bytes 165225 | solution.py:58
  188.2 4.4 all-to-all-start
  192.6 6.7 %all-to-all-done = bf16[4,128,256]{2,1,0:T(8,128)(2,1)S(1)} async-done(((bf16[4,128,256]{2,1,0:T(8,128)(2,1)}), bf16[4,128,256]{2,1,0:T(8,128)(2,1)S(1)}, u32[]{:S(2)}, u32[]{:S(2)}) %all-to-all-start) | async-done | bytes 262176 | tf_op jit(solution)/shard_map/all_to_all | solution.py:231
  199.5 3.1 multiply_reduce_fusion.2
  205.8 2.3 gather_fusion
  208.3 33.6 %scatter_fusion = bf16[64,6,2048]{2,0,1:T(8,128)(2,1)S(1)} fusion(bf16[64,6,2048]{2,0,1:T(8,128)(2,1)S(1)} %broadcast_in_dim.40, s32[256]{0:T(256)S(1)} %bitcast.315, bf16[256,2048]{1,0:T(8,128)(2,1)} %gather_fusion), kind=kCustom, calls=%fused_computation.2 | custom fusion | bytes 3147776 | tf_op jit(solution)/shard_map/scatter | solution.py:171
  242.8 59.3 %all_to_all.29 = bf16[64,6,2048]{2,1,0:T(8,128)(2,1)S(1)} all-to-all(bf16[64,6,2048]{2,1,0:T(8,128)(2,1)S(1)} %copy.181), channel_id=1, replica_groups=mesh['sp_0'=8,'sp_1'=4,'sp_2'=2,'tp'=4] {'sp_0','sp_1','sp_2'}, dimensions={0} | all-to-all | bytes 3145728 | tf_op jit(solution)/shard_map/all_to_all | solution.py:239
  303.7 2.5 fusion.180
  306.3 4.9 convolution_convert_fusion.1
  311.1 55.2 %all-gather.12.cloned.1.call-done = bf16[1536,2048]{1,0:T(8,128)(2,1)} async-done(((bf16[384,2048]{1,0:T(8,128)(2,1)}), bf16[1536,2048]{1,0:T(8,128)(2,1)}) %all-gather.12.cloned.1.call-update) | async-done | bytes 6291472 | tf_op jit(solution)/shard_map/all_gather | solution.py:243
  366.4 5.0 fusion.32
  371.4 2.1 fusion.17
  373.5 4.5 convolution_convert_fusion
  378.1 7.6 %pad_maximum_fusion = bf16[4,512,2048]{2,1,0:T(8,128)(2,1)} fusion(bf16[4,128,2048]{2,1,0:T(8,128)(2,1)S(1)} %bitcast.316, bf16[4,384,2048]{2,1,0:T(8,128)(2,1)} %convolution_convert_fusion), kind=kLoop, calls=%fused_computation.32 | loop fusion | flops 16777216 | bytes 16777216 | tf_op jit(solution)/shard_map/concatenate | solution.py:259
  385.7 83.9 %reduce-scatter.2.cloned.1.call-done = bf16[512,2048]{1,0:T(8,128)(2,1)} async-done(((bf16[2048,2048]{1,0:T(8,128)(2,1)}), bf16[512,2048]{1,0:T(8,128)(2,1)}) %reduce-scatter.2.cloned.1.call-update) | async-done | bytes 2097168 | tf_op jit(solution)/shard_map/reduce_scatter | solution.py:258
  472.6 10.9 %all-to-all-start.2 = ((bf16[64,6,2048]{2,1,0:T(8,128)(2,1)}), bf16[64,6,2048]{2,1,0:T(8,128)(2,1)}, u32[]{:S(2)}, u32[]{:S(2)}) async-start(bf16[64,6,2048]{2,1,0:T(8,128)(2,1)} %reshape.770), calls=%async_computation.3 | async-start | bytes 4194304 | tf_op jit(solution)/shard_map/all_to_all | solution.py:269
  483.6 51.0 %all-to-all-done.2 = bf16[64,6,2048]{2,1,0:T(8,128)(2,1)} async-done(((bf16[64,6,2048]{2,1,0:T(8,128)(2,1)}), bf16[64,6,2048]{2,1,0:T(8,128)(2,1)}, u32[]{:S(2)}, u32[]{:S(2)}) %all-to-all-start.2) | async-done | bytes 1572896 | tf_op jit(solution)/shard_map/all_to_all | solution.py:269
  534.6 2.6 reshape.771
  537.2 2.3 gather_fusion.1
  539.6 2.4 reshape.813
  542.0 3.2 multiply_reduce_fusion
  (401 shorter events, 118.6 us)
Async XLA Ops:
  6.5 367.0 %copy-start = (bf16[1,256,2048]{2,1,0:T(8,128)(2,1)S(1)}, bf16[1,256,2048]{2,1,0:T(8,128)(2,1)}, u32[]{:S(2)}) copy-start(bf16[1,256,2048]{2,1,0:T(8,128)(2,1)} %param.42) | copy-start | bytes 3145732
  6.5 167.2 %all-gather.16.cloned.1.call-start = ((), (), s32[]{:S(2)}) async-start(), calls=%async_computation.7 | async-start | bytes 2263040 | tf_op jit(solution)/shard_map/all_gather | solution.py:26
  9.2 13.9 %copy-start.21 = (bf16[512,128]{1,0:T(8,128)(2,1)S(1)}, bf16[512,128]{1,0:T(8,128)(2,1)}, u32[]{:S(2)}) copy-start(bf16[512,128]{1,0:T(8,128)(2,1)} %param.27) | copy-start | bytes 393220
  9.2 14.1 %copy-start.22 = (bf16[512,128]{1,0:T(8,128)(2,1)S(1)}, bf16[512,128]{1,0:T(8,128)(2,1)}, u32[]{:S(2)}) copy-start(bf16[512,128]{1,0:T(8,128)(2,1)} %param.28) | copy-start | bytes 393220
  9.6 13.5 %copy-start.7 = (f32[512,128]{0,1:T(8,128)}, f32[512,128]{0,1:T(8,128)S(1)}, u32[]{:S(2)}) copy-start(f32[512,128]{0,1:T(8,128)S(1)} %get-tuple-element.357) | copy-start | bytes 786436
  9.6 60.2 %copy-start.9 = (f32[512,128]{0,1:T(8,128)}, f32[512,128]{0,1:T(8,128)S(1)}, u32[]{:S(2)}) copy-start(f32[512,128]{0,1:T(8,128)S(1)} %get-tuple-element.416) | copy-start | bytes 786436
  23.9 5.2 copy-start.15
  23.9 5.2 copy-start.16
  23.9 2.9 copy-start.13
  74.9 4.5 copy-start.12
  82.4 25.3 %copy-start.18 = (bf16[8,64,2,128]{3,2,1,0:T(2,128)(2,1)S(1)}, bf16[8,64,2,128]{3,2,1,0:T(2,128)(2,1)}, u32[]{:S(2)}) copy-start(bf16[8,64,2,128]{3,2,1,0:T(2,128)(2,1)} %reshape_reshape.8) | copy-start | bytes 786436
  83.2 26.8 %copy-start.26 = (s32[128,2]{0,1:T(2,128)S(1)}, s32[128,2]{0,1:T(2,128)}, u32[]{:S(2)}) copy-start(s32[128,2]{0,1:T(2,128)} %param.38) | copy-start | bytes 3076
  160.3 1.9 copy-start.10
  162.0 4.0 copy-start.11
  165.0 5.0 copy-start.8
  174.8 12.2 %copy-start.27 = (f32[256]{0:T(256)S(1)}, f32[256]{0:T(256)}, u32[]{:S(2)}) copy-start(f32[256]{0:T(256)} %param.33) | copy-start | bytes 3076
  185.2 2.1 copy-start.20
  188.2 11.1 %all-to-all-start = ((bf16[4,128,256]{2,1,0:T(8,128)(2,1)}), bf16[4,128,256]{2,1,0:T(8,128)(2,1)S(1)}, u32[]{:S(2)}, u32[]{:S(2)}) async-start(bf16[4,128,256]{2,1,0:T(8,128)(2,1)} %bitcast.62), calls=%async_computation | async-start | bytes 524288 | tf_op jit(solution)/shard_map/all_to_all | solution.py:231
  192.6 111.1 %all-gather.14.cloned.1.call-start = ((), (), s32[]{:S(2)}) async-start(), calls=%async_computation.5 | async-start | bytes 2621440 | tf_op jit(solution)/shard_map/all_gather | solution.py:244
  199.5 3.1 copy-start.19
  199.5 3.1 copy-start.23
  204.8 161.6 %all-gather.12.cloned.1.call-start = ((), (), s32[]{:S(2)}) async-start(), calls=%async_computation.4 | async-start | bytes 7864320 | tf_op jit(solution)/shard_map/all_gather | solution.py:243
  303.7 166.0 %reduce-scatter.2.cloned.1.call-start = ((), (), s32[]{:S(2)}) async-start(), calls=%async_computation.6 | async-start | bytes 10485760 | tf_op jit(solution)/shard_map/reduce_scatter | solution.py:258
  303.7 2.5 copy-start.2
  311.1 60.3 %copy-start.30 = (bf16[1,2048,256]{2,1,0:T(8,128)(2,1)S(1)}, bf16[1,2048,256]{2,1,0:T(8,128)(2,1)}, u32[]{:S(2)}) copy-start(bf16[1,2048,256]{2,1,0:T(8,128)(2,1)} %param.41) | copy-start | bytes 3145732
  366.4 5.1 copy-start.29
  373.5 4.5 copy-start.3
  472.6 10.9 %copy-start.28 = (f32[128,2]{0,1:T(2,128)S(1)}, f32[128,2]{0,1:T(2,128)}, u32[]{:S(2)}) copy-start(f32[128,2]{0,1:T(2,128)} %param.39) | copy-start | bytes 3076
  472.6 62.0 %all-to-all-start.2 = ((bf16[64,6,2048]{2,1,0:T(8,128)(2,1)}), bf16[64,6,2048]{2,1,0:T(8,128)(2,1)}, u32[]{:S(2)}, u32[]{:S(2)}) async-start(bf16[64,6,2048]{2,1,0:T(8,128)(2,1)} %reshape.770), calls=%async_computation.3 | async-start | bytes 4194304 | tf_op jit(solution)/shard_map/all_to_all | solution.py:269
  541.9 3.2 copy-start.4
  542.0 3.5 copy-start.6
  542.0 3.5 copy-start.25
  (7 other events, 7.5 us)
Sparse Core Ops, SparseCore 0:
  62.0 79.3 all-gather.15
  204.9 30.5 all-gather.13
  303.8 62.5 all-gather.11
  385.8 83.7 reduce-scatter.1
where the time goes:
time: 557 us; the launch traced here: 553 us
  waiting for transfers between devices  197 us (35%)
  local copies, waits for them, and re-layouts  119 us (21%)
  blocking collectives  102 us (18%)
  matrix products  56.2 us (10%)
  other arithmetic  46.9 us (8%)
  starting transfers between devices  15.3 us (3%)
  between operations  14 us (3%)
    reduce_scatter x1, waiting for transfers between devices, body(): lax.psum_scatter(jnp.concatenate([routed_out, shared_out], axis=1).reshap...  83.9 us
    all_to_all x1, blocking collectives, body(): lax.all_to_all(fill_slots(normed, routes, experts, capacity), SP, split_a...  59.3 us
    all_gather x1, waiting for transfers between devices, body(): lax.all_gather(arrived.reshape(experts * capacity, model_width), 'tp', ax...  55.2 us
    all_to_all x1, waiting for transfers between devices, body(): lax.all_to_all(routed_done, SP, split_axis=0, concat_axis=0, tiled=True)  51 us
    all_gather x3, blocking collectives, gathered_once(): both, at, found = (lax.all_gather(jnp.concatenate(lines), axis), 0, {})  42.6 us
    scatter x2, local copies, waits for them, and re-layouts, fill_slots(): return buffer.at[flat_ids, slot_ids].set(row_data[token_ids])  34.5 us
    dynamic_slice x32, local copies, waits for them, and re-layouts, blockwise(): lax.scan(advance, start_state, (query_in, key_out, value_blocks, block_de...  20.9 us
    dot_general x16, matrix products, advance(): jnp.einsum('jco,jcm->com', key_segment, value_segment)  15.2 us
  transfers between devices with their start and end apart: 6, of which 4 were waited for; matrix products, arithmetic and copies ran while one was open for 21% of the time, Pallas kernels for 0%

commit v1 on v0

--- a/solution.py
+++ b/solution.py
@@ -13,6 +13,14 @@
 EPS = 1e-06
 GATE_NORM = 16.0
 ROPE_BASE = 10000.0
+
+
+def tiled_gather(array, axis, dim):
+    count = lax.axis_size(axis)
+    repeats = [count if d == dim else 1 for d in range(array.ndim)]
+    return lax.all_to_all(
+        jnp.tile(array, repeats), axis, split_axis=dim, concat_axis=dim, tiled=True
+    )
 
 
 def gathered_once(array, axis):
@@ -240,7 +248,7 @@
         fill_slots(normed, routes, experts, capacity), SP, split_axis=0, concat_axis=0, tiled=True
     )
     fanned, shared_flat = (
-        lax.all_gather(arrived.reshape(experts * capacity, model_width), "tp", axis=0, tiled=True),
+        tiled_gather(arrived.reshape(experts * capacity, model_width), "tp", 0),
         lax.all_gather(normed, "tp", axis=0, tiled=True),
     )
     routed_rows = fanned.reshape(groups, experts * capacity, model_width)

time: 557 us -> 600 us (1.077)
  waiting for transfers between devices: 197 us -> 223 us
  local copies, waits for them, and re-layouts: 119 us -> 129 us
    all_gather x1 -> x0, waiting for transfers between devices: 55.2 us -> none  [body(): lax.all_gather(arrived.reshape(experts * capacity, model_width), 'tp', ax...]
    all_gather x1, waiting for transfers between devices: 0.02 us -> 48.6 us  [body(): lax.all_gather(normed, 'tp', axis=0, tiled=True)]
    all_to_all x0 -> x1, waiting for transfers between devices: none -> 30 us  [tiled_gather(): lax.all_to_all(jnp.tile(array, repeats), axis, split_axis=dim, concat_axi...]
    another operation x11 -> x13, local copies, waits for them, and re-layouts: 2.18 us -> 8.48 us  [the longest x2 6.29 us: tiled_gather(): jnp.tile(array, repeats)]
  transfers between devices with their start and end apart: 6 -> 6, of which waited for: 4 -> 5; matrix products, arithmetic and copies ran while one was open for 21% -> 14% of each run, Pallas kernels for 0% -> 0%
where the time goes in v1:
time: 600 us; the launch traced here: 596 us
  waiting for transfers between devices  223 us (37%)
  local copies, waits for them, and re-layouts  129 us (22%)
  blocking collectives  102 us (17%)
  matrix products  58.9 us (10%)
  other arithmetic  46.1 us (8%)
  starting transfers between devices  20.8 us (3%)
  between operations  14.2 us (2%)
    reduce_scatter x1, waiting for transfers between devices, body(): lax.psum_scatter(jnp.concatenate([routed_out, shared_out], axis=1).reshap...  85.7 us
    all_to_all x1, blocking collectives, body(): lax.all_to_all(fill_slots(normed, routes, experts, capacity), SP, split_a...  59.6 us
    all_to_all x1, waiting for transfers between devices, body(): lax.all_to_all(routed_done, SP, split_axis=0, concat_axis=0, tiled=True)  51 us
    all_gather x1, waiting for transfers between devices, body(): lax.all_gather(normed, 'tp', axis=0, tiled=True)  48.6 us
    all_gather x3, blocking collectives, gathered_once(): both, at, found = (lax.all_gather(jnp.concatenate(lines), axis), 0, {})  42.5 us
    scatter x2, local copies, waits for them, and re-layouts, fill_slots(): return buffer.at[flat_ids, slot_ids].set(row_data[token_ids])  34.5 us
    all_to_all x1, waiting for transfers between devices, tiled_gather(): lax.all_to_all(jnp.tile(array, repeats), axis, split_axis=dim, concat_axi...  30 us
    dynamic_slice x32, local copies, waits for them, and re-layouts, blockwise(): lax.scan(advance, start_state, (query_in, key_out, value_blocks, block_de...  20.8 us
  transfers between devices with their start and end apart: 6, of which 5 were waited for; matrix products, arithmetic and copies ran while one was open for 14% of the time, Pallas kernels for 0%

profile of v1, /device:TPU:2, one launch (start us, length us, event | category | flops | bytes accessed | tf_op | source)
XLA Modules:
  0.0 596.0 jit_solution(3797281658250425025)
XLA Ops:
  10.0 13.0 %fusion.178 = f32[8,64,2,64]{3,0,1,2:T(8,128)S(1)} fusion(f32[8,64,2,64]{3,0,1,2:T(8,128)S(1)} %copy.134), kind=kOutput, calls=%fused_computation.308 | output fusion | flops 4128768 | bytes 524288 | tf_op jit(solution)/shard_map/jit(cumsum)/reduce_window_sum | solution.py:124
  36.9 24.3 %while.40 = (s32[]{:T(128)}, f32[2,64,128]{2,1,0:T(8,128)S(1)}, f32[8,64,2,128]{3,1,2,0:T(8,128)}, f32[8,2,64]{2,0,1:T(8,128)S(1)}, f32[8,64,2,64]{3,0,1,2:T(8,1...) while((s32[]{:T(128)}, f32[2,64,128]{2,1,0:T(8,128)S(1)}, ...), condition=%wide.region_2.3_spmd.clone, body=%wide.region_1.2_spmd.clone.sunk | while | flops 4259843 | bytes 494192 | solution.py:145
  63.7 3.1 rev.15
  66.8 3.1 rev.17
  83.6 2.9 rev.18
  90.3 24.4 %while.42 = (s32[]{:T(128)}, f32[2,64,128]{2,1,0:T(8,128)S(1)}, f32[8,64,2,128]{3,1,2,0:T(8,128)}, f32[8,2,64]{2,0,1:T(8,128)S(1)}, f32[8,64,2,64]{3,0,1,2:T(8,1...) while((s32[]{:T(128)}, f32[2,64,128]{2,1,0:T(8,128)S(1)}, ...), condition=%wide.region_10.11_spmd.clone, body=%wide.region_9.10_spmd.clone.sunk | while | flops 4259843 | bytes 494192 | solution.py:145
  116.8 12.2 %all-gather.6 = bf16[4,129,128]{2,1,0:T(8,128)(2,1)S(1)} all-gather(bf16[1,129,128]{2,1,0:T(8,128)(2,1)S(1)} %maximum_bitcast_fusion.2), channel_id=4, replica_groups=mesh['sp_0'=8,'sp_1'=4,'sp_2'=2,'tp'=4] {'sp_1'}, dimensions={0}, use_global_device_ids=true | all-gather | bytes 165120 | tf_op jit(solution)/shard_map/all_gather | solution.py:34
  130.8 28.4 %all-gather.7 = bf16[8,129,128]{2,1,0:T(8,128)(2,1)S(1)} all-gather(bf16[1,129,128]{2,1,0:T(8,128)(2,1)S(1)} %maximum_bitcast_fusion.3), channel_id=5, replica_groups=mesh['sp_0'=8,'sp_1'=4,'sp_2'=2,'tp'=4] {'sp_0'}, dimensions={0}, use_global_device_ids=true | all-gather | bytes 297216 | tf_op jit(solution)/shard_map/all_gather | solution.py:34
  168.1 2.4 reduce-window.24
  172.7 3.0 rev.19
  175.8 2.4 reduce-window.20
  182.2 8.8 %while.41 = (s32[]{:T(128)}, f32[2,64,128]{2,1,0:T(8,128)S(1)}, s32[]{:T(128)}, bf16[64,2,64]{2,1,0:T(2,128)(2,1)S(1)}, bf16[64,2,64,128]{3,2,1,0:T(8,128)(2,1)S(1)}, /*index=5*/s32[]{:T(128)}, s32[]{:T(128)}) while((s32[]{:T(128)}, f32[2,64,128]{2,1,0:T(8,128)S(1)}, s32[]{:T(128)}, bf16[64,2,64]{2,1,0:T(2,128)(2,1)S(1)}, ...), condition=%wide.region_5.6_spmd.clone, body=%wide.region_4.5_spmd.clone.sunk | while | flops 82052 | bytes 165225 | solution.py:66
  194.0 4.4 all-to-all-start
  198.4 6.7 %all-to-all-done = bf16[4,128,256]{2,1,0:T(8,128)(2,1)S(1)} async-done(((bf16[4,128,256]{2,1,0:T(8,128)(2,1)}), bf16[4,128,256]{2,1,0:T(8,128)(2,1)S(1)}, u32[]{:S(2)}, u32[]{:S(2)}) %all-to-all-start) | async-done | bytes 262176 | tf_op jit(solution)/shard_map/all_to_all | solution.py:239
  205.3 3.1 multiply_reduce_fusion.2
  212.3 33.6 %scatter_fusion = bf16[64,6,2048]{2,0,1:T(8,128)(2,1)S(1)} fusion(bf16[64,6,2048]{2,0,1:T(8,128)(2,1)S(1)} %broadcast_in_dim.40, s32[256]{0:T(256)S(1)} %bitcast.316, bf16[256,2048]{1,0:T(8,128)(2,1)} %gather_fusion), kind=kCustom, calls=%fused_computation.2 | custom fusion | bytes 3147776 | tf_op jit(solution)/shard_map/scatter | solution.py:179
  246.8 59.6 %all_to_all.38 = bf16[64,6,2048]{2,1,0:T(8,128)(2,1)S(1)} all-to-all(bf16[64,6,2048]{2,1,0:T(8,128)(2,1)S(1)} %copy.181), channel_id=1, replica_groups=mesh['sp_0'=8,'sp_1'=4,'sp_2'=2,'tp'=4] {'sp_0','sp_1','sp_2'}, dimensions={0} | all-to-all | bytes 3145728 | tf_op jit(solution)/shard_map/all_to_all | solution.py:247
  307.8 4.9 tile.9
  312.7 5.2 all-to-all-start.2
  318.9 48.6 %all-gather.11.cloned.1.call-done = bf16[512,2048]{1,0:T(8,128)(2,1)} async-done(((bf16[128,2048]{1,0:T(8,128)(2,1)}), bf16[512,2048]{1,0:T(8,128)(2,1)}) %all-gather.11.cloned.1.call-update) | async-done | bytes 2097168 | tf_op jit(solution)/shard_map/all_gather | solution.py:252
  367.5 2.5 fusion.180
  370.0 4.8 convolution_convert_fusion.1
  374.9 30.0 %all-to-all-done.2 = bf16[4,384,2048]{2,1,0:T(8,128)(2,1)} async-done(((bf16[4,384,2048]{2,1,0:T(8,128)(2,1)}), bf16[4,384,2048]{2,1,0:T(8,128)(2,1)}, u32[]{:S(2)}, u32[]{:S(2)}) %all-to-all-start.2) | async-done | bytes 6291488 | tf_op jit(solution)/shard_map/all_to_all | solution.py:21
  404.8 5.0 fusion.32
  409.9 4.8 fusion.17
  414.7 4.5 convolution_convert_fusion
  419.2 7.6 %pad_maximum_fusion = bf16[4,512,2048]{2,1,0:T(8,128)(2,1)} fusion(bf16[4,128,2048]{2,1,0:T(8,128)(2,1)S(1)} %bitcast.317, bf16[4,384,2048]{2,1,0:T(8,128)(2,1)} %convolution_convert_fusion), kind=kLoop, calls=%fused_computation.32 | loop fusion | flops 16777216 | bytes 16777216 | tf_op jit(solution)/shard_map/concatenate | solution.py:267
  426.9 85.7 %reduce-scatter.2.cloned.1.call-done = bf16[512,2048]{1,0:T(8,128)(2,1)} async-done(((bf16[2048,2048]{1,0:T(8,128)(2,1)}), bf16[512,2048]{1,0:T(8,128)(2,1)}) %reduce-scatter.2.cloned.1.call-update) | async-done | bytes 2097168 | tf_op jit(solution)/shard_map/reduce_scatter | solution.py:266
  515.6 10.9 %all-to-all-start.3 = ((bf16[64,6,2048]{2,1,0:T(8,128)(2,1)}), bf16[64,6,2048]{2,1,0:T(8,128)(2,1)}, u32[]{:S(2)}, u32[]{:S(2)}) async-start(bf16[64,6,2048]{2,1,0:T(8,128)(2,1)} %reshape.773), calls=%async_computation.4 | async-start | bytes 4194304 | tf_op jit(solution)/shard_map/all_to_all | solution.py:277
  526.5 51.0 %all-to-all-done.3 = bf16[64,6,2048]{2,1,0:T(8,128)(2,1)} async-done(((bf16[64,6,2048]{2,1,0:T(8,128)(2,1)}), bf16[64,6,2048]{2,1,0:T(8,128)(2,1)}, u32[]{:S(2)}, u32[]{:S(2)}) %all-to-all-start.3) | async-done | bytes 1572896 | tf_op jit(solution)/shard_map/all_to_all | solution.py:277
  577.6 2.6 reshape.774
  584.9 3.2 multiply_reduce_fusion
  (425 shorter events, 129.8 us)
Async XLA Ops:
  6.5 408.2 %copy-start = (bf16[1,256,2048]{2,1,0:T(8,128)(2,1)S(1)}, bf16[1,256,2048]{2,1,0:T(8,128)(2,1)}, u32[]{:S(2)}) copy-start(bf16[1,256,2048]{2,1,0:T(8,128)(2,1)} %param.42) | copy-start | bytes 3145732
  6.5 173.0 %all-gather.13.cloned.1.call-start = ((), (), s32[]{:S(2)}) async-start(), calls=%async_computation.7 | async-start | bytes 2263040 | tf_op jit(solution)/shard_map/all_gather | solution.py:34
  9.2 13.9 %copy-start.23 = (bf16[512,128]{1,0:T(8,128)(2,1)S(1)}, bf16[512,128]{1,0:T(8,128)(2,1)}, u32[]{:S(2)}) copy-start(bf16[512,128]{1,0:T(8,128)(2,1)} %param.27) | copy-start | bytes 393220
  9.2 14.1 %copy-start.24 = (bf16[512,128]{1,0:T(8,128)(2,1)S(1)}, bf16[512,128]{1,0:T(8,128)(2,1)}, u32[]{:S(2)}) copy-start(bf16[512,128]{1,0:T(8,128)(2,1)} %param.28) | copy-start | bytes 393220
  9.6 13.5 %copy-start.7 = (f32[512,128]{0,1:T(8,128)}, f32[512,128]{0,1:T(8,128)S(1)}, u32[]{:S(2)}) copy-start(f32[512,128]{0,1:T(8,128)S(1)} %get-tuple-element.357) | copy-start | bytes 786436
  9.6 60.3 %copy-start.9 = (f32[512,128]{0,1:T(8,128)}, f32[512,128]{0,1:T(8,128)S(1)}, u32[]{:S(2)}) copy-start(f32[512,128]{0,1:T(8,128)S(1)} %get-tuple-element.416) | copy-start | bytes 786436
  23.9 5.2 copy-start.15
  23.9 5.2 copy-start.16
  63.7 11.0 %copy-start.33 = (s32[128,2]{0,1:T(2,128)S(1)}, s32[128,2]{0,1:T(2,128)}, u32[]{:S(2)}) copy-start(s32[128,2]{0,1:T(2,128)} %param.38) | copy-start | bytes 3076
  80.0 3.5 copy-start.12
  90.3 74.8 %copy-start.25 = (f32[8,2,64]{2,0,1:T(8,128)S(1)}, f32[8,2,64]{2,0,1:T(8,128)}, u32[]{:S(2)}) copy-start(f32[8,2,64]{2,0,1:T(8,128)} %get-tuple-element.374) | copy-start | bytes 12292
  129.0 36.1 %copy-start.17 = (bf16[4,129,128]{2,1,0:T(8,128)(2,1)}, bf16[4,129,128]{2,1,0:T(8,128)(2,1)S(1)}, u32[]{:S(2)}) copy-start(bf16[4,129,128]{2,1,0:T(8,128)(2,1)S(1)} %all-gather.6) | copy-start | bytes 396292
  129.9 40.9 %copy-start.31 = (f32[2,64]{1,0:T(2,128)}, f32[2,64]{1,0:T(2,128)S(1)}, u32[]{:S(2)}) copy-start(f32[2,64]{1,0:T(2,128)S(1)} %reshape.807) | copy-start | bytes 1540
  130.6 40.2 %copy-start.32 = (f32[2,64]{1,0:T(2,128)}, f32[2,64]{1,0:T(2,128)S(1)}, u32[]{:S(2)}) copy-start(f32[2,64]{1,0:T(2,128)S(1)} %reshape.809) | copy-start | bytes 1540
  167.8 3.2 copy-start.18
  167.8 3.2 copy-start.36
  167.8 3.2 copy-start.37
  170.9 4.8 copy-start.8
  171.0 7.4 %copy-start.29 = (s32[2,128]{1,0:T(2,128)S(1)}, s32[2,128]{1,0:T(2,128)}, u32[]{:S(2)}) copy-start(s32[2,128]{1,0:T(2,128)} %eq.36) | copy-start | bytes 3076
  180.6 12.2 %copy-start.34 = (f32[256]{0:T(256)S(1)}, f32[256]{0:T(256)}, u32[]{:S(2)}) copy-start(f32[256]{0:T(256)} %param.33) | copy-start | bytes 3076
  192.8 5.6 copy-start.30
  194.0 11.1 %all-to-all-start = ((bf16[4,128,256]{2,1,0:T(8,128)(2,1)}), bf16[4,128,256]{2,1,0:T(8,128)(2,1)S(1)}, u32[]{:S(2)}, u32[]{:S(2)}) async-start(bf16[4,128,256]{2,1,0:T(8,128)(2,1)} %bitcast.62), calls=%async_computation | async-start | bytes 524288 | tf_op jit(solution)/shard_map/all_to_all | solution.py:239
  312.7 92.2 %all-to-all-start.2 = ((bf16[4,384,2048]{2,1,0:T(8,128)(2,1)}), bf16[4,384,2048]{2,1,0:T(8,128)(2,1)}, u32[]{:S(2)}, u32[]{:S(2)}) async-start(bf16[4,384,2048]{2,1,0:T(8,128)(2,1)} %tile.9), calls=%async_computation.2 | async-start | bytes 12582912 | tf_op jit(solution)/shard_map/all_to_all | solution.py:21
  317.9 49.6 %all-gather.11.cloned.1.call-start = ((), (), s32[]{:S(2)}) async-start(), calls=%async_computation.5 | async-start | bytes 2621440 | tf_op jit(solution)/shard_map/all_gather | solution.py:252
  318.6 193.9 %reduce-scatter.2.cloned.1.call-start = ((), (), s32[]{:S(2)}) async-start(), calls=%async_computation.6 | async-start | bytes 10485760 | tf_op jit(solution)/shard_map/reduce_scatter | solution.py:266
  404.8 5.0 copy-start.42
  414.7 4.5 copy-start.3
  515.6 10.9 %copy-start.35 = (f32[128,2]{0,1:T(2,128)S(1)}, f32[128,2]{0,1:T(2,128)}, u32[]{:S(2)}) copy-start(f32[128,2]{0,1:T(2,128)} %param.39) | copy-start | bytes 3076
  515.6 62.0 %all-to-all-start.3 = ((bf16[64,6,2048]{2,1,0:T(8,128)(2,1)}), bf16[64,6,2048]{2,1,0:T(8,128)(2,1)}, u32[]{:S(2)}, u32[]{:S(2)}) async-start(bf16[64,6,2048]{2,1,0:T(8,128)(2,1)} %reshape.773), calls=%async_computation.4 | async-start | bytes 4194304 | tf_op jit(solution)/shard_map/all_to_all | solution.py:277
  584.9 3.2 copy-start.4
  584.9 3.5 copy-start.6
  584.9 3.5 copy-start.28
  (19 other events, 43.2 us)
Sparse Core Ops, SparseCore 0:
  62.0 79.5 all-gather.12
  320.5 46.9 all-gather.10
  427.0 85.5 reduce-scatter.1
